TPU v7x, 32 devices: a whole 2x2x4 slice. The times are simulated.
32 devices in a mesh: grp: 2 (over y), sp: 4 (over z), tp: 4 (over x, core).
Axes of the slice: x: 2, y: 2, z: 4, core: 2. Of those that a mesh axis runs over, the one named last changes fastest.
Arguments:
- latent: bfloat16 [4096, 4096], P(('grp', 'sp'), 'tp'), parts along dimension 0, may hold values from -42 to 42
- context: bfloat16 [2048, 4096], P(('grp', 'sp'), 'tp'), parts along dimension 0, may hold values from -42 to 42
- conditions: float32 [4, 4096], P('grp', 'sp'), parts along dimension 0, may hold values from -6 to 6
- mod_weight: bfloat16 [4096, 3, 4096], P('sp', None, 'tp'), may hold values from -0.09375 to 0.09375
- norm_gain: float32 [4096], P('tp'), may hold values from 0.1 to 1.9
- w_query: bfloat16 [4096, 2048], P(None, 'tp'), may hold values from -0.09375 to 0.09375
- w_key: bfloat16 [4096, 2048], P(None, 'tp'), may hold values from -0.09375 to 0.09375
- w_value: bfloat16 [4096, 2048], P(None, 'tp'), may hold values from -0.09375 to 0.09375
- query_gain: float32 [64], replicated, may hold values from 1 to 14
- key_gain: float32 [64], replicated, may hold values from 1 to 14
- lambdas: float32 [16], P('tp'), may hold values from 0.3 to 0.8
- out_gain: float32 [128], replicated, may hold values from 0.1 to 1.9
- w_out: bfloat16 [2048, 4096], P(None, 'tp'), may hold values from -0.125 to 0.125
Outputs:
- updated: bfloat16 [4096, 4096], P(('grp', 'sp'), 'tp'), parts along dimension 0
There are 2 independent parts, one for each index of `grp`. A program takes and returns all parts, laid end to end along the dimension named above; an argument that names none is the same for every part. Nothing has to cross between parts.
All inputs are finite; a program needn't handle non-finite values.
Results may differ from a plain program's by a relative error of at most 0.0076.
Values may be sent and summed in bfloat16 or wider, within the bound.
A program may use at most 128 MiB of HBM per device.

v0:
```python
import math
import jax
import jax.numpy as jnp
from jax import lax
from jax.sharding import PartitionSpec as P

DK = 64
DV = 128
GRID_W = 64
epsilon = 1e-06


def turn_half(halves, angles):
    quarter = halves.shape[-1] // 2
    cosine = jnp.cos(angles)[:, None, None, :]
    sine_part = jnp.sin(angles)[:, None, None, :]
    first_part = halves[..., :quarter]
    second = halves[..., quarter:]
    return jnp.concatenate(
        [first_part * cosine - second * sine_part, first_part * sine_part + second * cosine],
        axis=-1,
    )


def rotate(features, positions):
    half_width = features.shape[-1] // 2
    quarter = half_width // 2
    inverse = 10000.0 ** (-2.0 * jnp.arange(quarter, dtype=jnp.float32) / half_width)
    grid_row = (positions // GRID_W).astype(jnp.float32)
    grid_column = (positions % GRID_W).astype(jnp.float32)
    return jnp.concatenate(
        [
            turn_half(features[..., :half_width], grid_row[:, None] * inverse),
            turn_half(features[..., half_width:], grid_column[:, None] * inverse),
        ],
        axis=-1,
    )


def head_norm(features, gain_row):
    return (
        features
        * lax.rsqrt(jnp.mean(features * features, axis=-1, keepdims=True) + epsilon)
        * gain_row
    )


def modulate(rows_in, gain_row, shift_row, scale_row):
    floats = rows_in.astype(jnp.float32)
    factor = lax.rsqrt(jnp.mean(floats * floats, axis=1, keepdims=True) + epsilon)
    return (floats * factor * gain_row * (1.0 + scale_row) + shift_row).astype(jnp.bfloat16)


def local(
    latent,
    context,
    conditions,
    mod_weight,
    norm_gain,
    w_query,
    w_key,
    w_value,
    query_gain,
    key_gain,
    lambdas,
    out_gain,
    w_out,
):
    tok_rows = latent.shape[0]
    ctx_rows = context.shape[0]
    columns = latent.shape[1]
    heads_here = lambdas.shape[0]
    in_rows = mod_weight.shape[0]
    activated = jax.nn.silu(conditions).astype(jnp.bfloat16)
    partial_mod = jnp.dot(
        activated, mod_weight.reshape(in_rows, 3 * columns), preferred_element_type=jnp.float32
    ).reshape(2, 3, columns)
    modulation = lax.psum(partial_mod, "sp")
    lat_floats = latent.astype(jnp.float32)
    full_gain, full_pairs = (
        lax.all_gather(norm_gain, "tp", axis=0, tiled=True),
        lax.all_gather(modulation[:, :2], "tp", axis=2, tiled=True),
    )
    whole_lat, whole_ctx = (
        lax.all_gather(latent, "tp", axis=1, tiled=True),
        lax.all_gather(context, "tp", axis=1, tiled=True),
    )
    hidden = modulate(whole_lat, full_gain, full_pairs[0, 0], full_pairs[0, 1])
    hidden_ctx = modulate(whole_ctx, full_gain, full_pairs[1, 0], full_pairs[1, 1])
    query_raw = jnp.dot(hidden, w_query, preferred_element_type=jnp.float32)
    key_raw = jnp.dot(hidden, w_key, preferred_element_type=jnp.float32)
    value_raw = jnp.dot(hidden, w_value, preferred_element_type=jnp.float32)
    ctx_key_raw = jnp.dot(hidden_ctx, w_key, preferred_element_type=jnp.float32)
    ctx_value_raw = jnp.dot(hidden_ctx, w_value, preferred_element_type=jnp.float32)
    positions = lax.axis_index("sp") * tok_rows + jnp.arange(tok_rows, dtype=jnp.int32)
    queries = rotate(
        head_norm(query_raw.reshape(tok_rows, heads_here, 2, DK), query_gain), positions
    ).astype(jnp.bfloat16)
    lat_keys = (
        rotate(head_norm(key_raw.reshape(tok_rows, heads_here, 2, DK), key_gain), positions)
        .astype(jnp.bfloat16)
        .reshape(tok_rows, heads_here * 2 * DK)
    )
    lat_values = value_raw.astype(jnp.bfloat16)
    ctx_keys = (
        head_norm(ctx_key_raw.reshape(ctx_rows, heads_here, 2, DK), key_gain)
        .astype(jnp.bfloat16)
        .reshape(ctx_rows, heads_here * 2 * DK)
    )
    ctx_values = ctx_value_raw.astype(jnp.bfloat16)
    scaling = DK ** (-0.5)

    def absorb(carried, key_rows, value_rows):
        key_count = key_rows.shape[0]
        key_block = key_rows.reshape(key_count, heads_here, 2, DK)
        value_block = value_rows.reshape(key_count, heads_here, DV)
        running_max, totals, weighted = carried
        scores = (
            jnp.einsum("qhmd,khmd->qhmk", queries, key_block, preferred_element_type=jnp.float32)
            * scaling
        )
        new_max = jnp.maximum(running_max, jnp.max(scores, axis=-1))
        rescale = jnp.exp(running_max - new_max)
        exponent = jnp.exp(scores - new_max[..., None])
        totals = totals * rescale + jnp.sum(exponent, axis=-1)
        weighted = weighted * rescale[..., None] + jnp.einsum(
            "qhmk,khv->qhmv",
            exponent.astype(jnp.bfloat16),
            value_block,
            preferred_element_type=jnp.float32,
        )
        return (new_max, totals, weighted)

    def absorb_rows(carried, key_rows, value_rows):
        key_count = key_rows.shape[0]
        block_rows = math.gcd(key_count, 512)

        def visit_block(block_index, partial_value):
            first_row = block_index * block_rows
            return absorb(
                partial_value,
                lax.dynamic_slice_in_dim(key_rows, first_row, block_rows, 0),
                lax.dynamic_slice_in_dim(value_rows, first_row, block_rows, 0),
            )

        return lax.fori_loop(0, key_count // block_rows, visit_block, carried)

    initial_state = (
        jnp.full((tok_rows, heads_here, 2), -1e30, jnp.float32),
        jnp.zeros((tok_rows, heads_here, 2), jnp.float32),
        jnp.zeros((tok_rows, heads_here, 2, DV), jnp.float32),
    )
    every_ctx_keys, every_ctx_values = (
        lax.all_gather(ctx_keys, "sp", axis=0, tiled=True),
        lax.all_gather(ctx_values, "sp", axis=0, tiled=True),
    )
    carried = absorb_rows(initial_state, every_ctx_keys, every_ctx_values)
    carried = absorb_rows(
        carried,
        lax.all_gather(lat_keys, "sp", axis=0, tiled=True),
        lax.all_gather(lat_values, "sp", axis=0, tiled=True),
    )
    running_max, totals, weighted = carried
    attended = (
        weighted[:, :, 0] / totals[:, :, 0, None]
        - lambdas[None, :, None] * weighted[:, :, 1] / totals[:, :, 1, None]
    )
    head_out = head_norm(attended, out_gain).astype(jnp.bfloat16).reshape(tok_rows, heads_here * DV)
    mixed_rows = jnp.dot(
        lax.all_gather(head_out, "tp", axis=1, tiled=True),
        w_out,
        preferred_element_type=jnp.float32,
    )
    return (lat_floats + modulation[0, 2] * mixed_rows).astype(jnp.bfloat16)


def solution(mesh):
    in_specs = (
        P(("grp", "sp"), "tp"),
        P(("grp", "sp"), "tp"),
        P("grp", "sp"),
        P("sp", None, "tp"),
        P("tp"),
        P(None, "tp"),
        P(None, "tp"),
        P(None, "tp"),
        P(),
        P(),
        P("tp"),
        P(),
        P(None, "tp"),
    )
    out_specs = P(("grp", "sp"), "tp")
    return jax.shard_map(local, mesh=mesh, in_specs=in_specs, out_specs=out_specs, check_vma=False)
```

profile of v0, /device:TPU:0, one launch (start us, length us, event | category | flops | bytes accessed | tf_op | source)
XLA Modules:
  0.0 294.6 jit_solution(11514742589361231051)
XLA Ops:
  8.8 8.6 %copy.31 = bf16[1024,3,1024]{0,2,1:T(8,128)(2,1)} copy(bf16[1024,3,1024]{2,0,1:T(8,128)(2,1)} %param.20) | data formatting | bytes 12582912 | tf_op args[3]
  17.5 5.1 %fusion.27 = f32[2,3,1024]{2,0,1:T(2,128)S(1)} fusion(bf16[1024,3,1024]{0,2,1:T(8,128)(2,1)} %copy.31, f32[2,1024]{1,0:T(2,128)S(1)} %copy-done.4), kind=kOutput, calls=%fused_computation.39 | convolution fusion | flops 12593152 | bytes 6324224 | tf_op jit(solution)/shard_map/dot_general | solution.py:75
  22.5 20.6 %psum.7 = f32[2,3,1024]{2,0,1:T(2,128)S(1)} all-reduce(f32[2,3,1024]{2,0,1:T(2,128)S(1)} %fusion.27), channel_id=1, replica_groups=mesh['grp'=2,'sp'=4,'tp'=4] {'sp'}, use_global_device_ids=true, to_apply=%region_0.1 | all-reduce | flops 6144 | bytes 49152 | tf_op jit(solution)/shard_map/psum | solution.py:78
  43.2 5.2 %all_gather.28 = f32[4096]{0:T(1024)S(1)} all-gather(f32[1024]{0:T(1024)S(1)} %copy-done.7), channel_id=1, replica_groups=mesh['grp'=2,'sp'=4,'tp'=4] {'tp'}, dimensions={0}, use_global_device_ids=true | all-gather | bytes 20480 | tf_op jit(solution)/shard_map/all_gather | solution.py:81
  48.4 5.6 %all_gather.29 = f32[2,2,4096]{2,0,1:T(2,128)S(1)} all-gather(f32[2,2,1024]{2,0,1:T(2,128)S(1)} %slice.85), channel_id=1, replica_groups=mesh['grp'=2,'sp'=4,'tp'=4] {'tp'}, dimensions={2}, use_global_device_ids=true | all-gather | bytes 81920 | tf_op jit(solution)/shard_map/all_gather | solution.py:82
  54.1 2.1 fusion.29
  56.2 4.9 %convolution_convert_fusion.1 = bf16[256,512]{1,0:T(8,128)(2,1)} fusion(bf16[4096,512]{1,0:T(8,128)(2,1)} %param.24, bf16[256,4096]{1,0:T(8,128)(2,1)} %all-gather.8.cloned.1.call-done, f32[4096]{0:T(1024)S(1)} %bitcast.202, f32[4096]{0:T(1024)S(1)} %bitcast.204, f32[4096]{0:T(1024)S(1)} %all_gather.28, f32[256]{0:T(256)S(1)} %add_rsqrt_fusion.5), kind=kOutput, calls=%fused_computation.50 | convolution fusion | flops 1080164352 | bytes 6603776 | tf_op jit(solution)/shard_map/dot_general | solution.py:94
  61.4 5.0 %fusion.59 = (f32[256,512]{1,0:T(8,128)S(1)}, f32[256,512]{1,0:T(8,128)}) fusion(bf16[4096,512]{1,0:T(8,128)(2,1)} %param.23, bf16[256,4096]{1,0:T(8,128)(2,1)} %all-gather.8.cloned.1.call-done, f32[4096]{0:T(1024)S(1)} %bitcast.203, f32[4096]{0:T(1024)S(1)} %bitcast.205, f32[4096]{0:T(1024)S(1)} %all_gather.28, f32[256]{0:T(256)S(1)} %add_rsqrt_fusion.5), kind=kOutput, calls=%fused_computation.117 | convolution fusion | flops 1080164352 | bytes 7390208 | tf_op jit(solution)/shard_map/dot_general | solution.py:93
  66.9 1.9 multiply_convert_fusion
  70.7 3.2 %fusion.22 = f32[512]{0:T(512)S(1)} fusion(bf16[512,4096]{1,0:T(8,128)(2,1)} %all-gather.12.cloned.1.call-done), kind=kLoop, calls=%fused_computation.34 | loop fusion | flops 6290944 | bytes 4196352 | tf_op jit(solution)/shard_map/reduce_sum | solution.py:50
  74.1 5.4 %convolution_convert_fusion = bf16[512,512]{1,0:T(8,128)(2,1)} fusion(bf16[4096,512]{1,0:T(8,128)(2,1)} %param.24, bf16[512,4096]{1,0:T(8,128)(2,1)S(1)} %copy-done, f32[4096]{0:T(1024)S(1)} %bitcast.199, f32[4096]{0:T(1024)S(1)} %bitcast.196, f32[4096]{0:T(1024)S(1)} %all_gather.28, f32[512]{0:T(512)S(1)} %add_rsqrt_fusion.4), kind=kOutput, calls=%fused_computation.49 | convolution fusion | flops 2160328704 | bytes 8964096 | tf_op jit(solution)/shard_map/dot_general | solution.py:92
  79.8 6.4 %multiply_reduce_fusion = (f32[512,4,2]{0,2,1:T(2,128)S(1)}, f32[512,512]{0,1:T(8,128)S(1)}) fusion(bf16[4096,512]{1,0:T(8,128)(2,1)} %param.23, bf16[512,4096]{1,0:T(8,128)(2,1)} %all-gather.12.cloned.1.call-done, f32[4096]{0:T(1024)S(1)} %bitcast.200, f32[4096]{0:T(1024)S(1)} %bitcast.197, f32[4096]{0:T(1024)S(1)} %all_gather.28, f32[512]{0:T(512)S(1)} %add_rsqrt_fusion.4), kind=kOutput, calls=%fused_computation.64 | convolution fusion | flops 2160586752 | bytes 9504768 | tf_op jit(solution)/shard_map/dot_general | solution.py:91
  88.6 2.8 multiply_reduce_fusion.1
  92.2 8.0 %all-gather.14.cloned.1.call-done = bf16[1024,512]{1,0:T(8,128)(2,1)} async-done(((bf16[256,512]{1,0:T(8,128)(2,1)}), bf16[1024,512]{1,0:T(8,128)(2,1)}) %all-gather.14.cloned.1.call-update) | async-done | bytes 1048592 | tf_op jit(solution)/shard_map/all_gather | solution.py:155
  100.2 28.8 %all-gather.10.cloned.1.call-done = bf16[1024,512]{1,0:T(8,128)(2,1)} async-done(((bf16[256,512]{1,0:T(8,128)(2,1)}), bf16[1024,512]{1,0:T(8,128)(2,1)}) %all-gather.10.cloned.1.call-update) | async-done | bytes 1048592 | tf_op jit(solution)/shard_map/all_gather | solution.py:154
  129.0 20.6 %while.36 = (s32[]{:T(128)}, f32[512,4,2]{0,2,1:T(2,128)S(1)}, f32[512,4,2]{0,2,1:T(2,128)S(1)}, f32[512,4,2,128]{0,3,2,1:T(8,128)S(1)}, bf16[1024,512]{1,0:T(8,...) while((s32[]{:T(128)}, f32[512,4,2]{0,2,1:T(2,128)S(1)}, ...), condition=%wide.region_8.9_spmd.clone, body=%wide.region_5.8_spmd.clone.sunk | while | flops 823676928 | bytes 35389616 | solution.py:146
  129.0 2.1 constant_dynamic-slice_fusion.9
  132.1 1.3 copy.58
  133.3 2.4 bitcast_reduce_fusion.6
  135.7 1.4 fusion.96
  137.2 2.1 bitcast_add_fusion.5
  139.3 2.1 constant_dynamic-slice_fusion.9
  142.4 1.3 copy.58
  143.7 2.4 bitcast_reduce_fusion.6
  146.1 1.4 fusion.96
  147.5 2.1 bitcast_add_fusion.5
  149.7 25.8 %all-gather.18.cloned.1.call-done = bf16[2048,512]{1,0:T(8,128)(2,1)} async-done(((bf16[512,512]{1,0:T(8,128)(2,1)}), bf16[2048,512]{1,0:T(8,128)(2,1)}) %all-gather.18.cloned.1.call-update) | async-done | bytes 2097168 | tf_op jit(solution)/shard_map/all_gather | solution.py:161
  175.5 45.9 %all-gather.16.cloned.1.call-done = bf16[2048,512]{0,1:T(8,128)(2,1)} async-done(((bf16[512,512]{0,1:T(8,128)(2,1)}), bf16[2048,512]{0,1:T(8,128)(2,1)}) %all-gather.16.cloned.1.call-update) | async-done | bytes 2097168 | tf_op jit(solution)/shard_map/all_gather | solution.py:160
  221.4 36.4 %while.35 = (s32[]{:T(128)}, f32[512,4,2]{0,2,1:T(2,128)S(1)}, f32[512,4,2]{0,2,1:T(2,128)S(1)}, f32[512,4,2,128]{0,3,2,1:T(8,128)S(1)}, bf16[2048,512]{0,1:T(8,...) while((s32[]{:T(128)}, f32[512,4,2]{0,2,1:T(2,128)S(1)}, ...), condition=%wide.region_13.14_spmd, body=%wide.region_10.13_spmd.sunk | while | flops 823140352 | bytes 34341024 | solution.py:146
  221.4 1.9 constant_dynamic-slice_fusion.8
  223.3 1.3 copy.56
  225.6 1.3 bitcast_reduce_fusion.5
  227.0 1.4 fusion.90
  228.4 2.1 bitcast_add_fusion.4
  230.5 1.9 constant_dynamic-slice_fusion.8
  234.7 1.3 bitcast_reduce_fusion.5
  236.1 1.4 fusion.90
  237.5 2.1 bitcast_add_fusion.4
  239.6 1.9 constant_dynamic-slice_fusion.8
  243.9 1.3 bitcast_reduce_fusion.5
  245.2 1.4 fusion.90
  246.6 2.1 bitcast_add_fusion.4
  248.8 1.9 constant_dynamic-slice_fusion.8
  253.0 1.3 bitcast_reduce_fusion.5
  254.3 1.4 fusion.90
  255.7 2.1 bitcast_add_fusion.4
  260.8 20.8 %all-gather.20.cloned.1.call-done = bf16[512,2048]{0,1:T(8,128)(2,1)} async-done(((bf16[512,512]{0,1:T(8,128)(2,1)}), bf16[512,2048]{0,1:T(8,128)(2,1)}) %all-gather.20.cloned.1.call-update) | async-done | bytes 2097168 | tf_op jit(solution)/shard_map/all_gather | solution.py:170
  281.6 6.1 %add_convert_fusion = bf16[512,1024]{1,0:T(8,128)(2,1)} fusion(bf16[512,1024]{1,0:T(8,128)(2,1)S(1)} %copy-done.2, bf16[512,2048]{0,1:T(8,128)(2,1)} %all-gather.20.cloned.1.call-done, bf16[2048,1024]{1,0:T(8,128)(2,1)} %param.29, f32[1024]{0:T(1024)S(1)} %bitcast.206), kind=kOutput, calls=%fused_computation.48 | convolution fusion | flops 2149580800 | bytes 8392704 | tf_op jit(solution)/shard_map/dot_general | solution.py:169
  (107 shorter events, 21.9 us)
Async XLA Ops:
  6.5 47.5 %all-gather.8.cloned.1.call-start = ((), (), s32[]{:S(2)}) async-start(), calls=%async_computation | async-start | bytes 2621440 | tf_op jit(solution)/shard_map/all_gather | solution.py:86
  7.3 63.4 %all-gather.12.cloned.1.call-start = ((), (), s32[]{:S(2)}) async-start(), calls=%async_computation.2 | async-start | bytes 5242880 | tf_op jit(solution)/shard_map/all_gather | solution.py:85
  8.0 92.2 %all-gather.14.cloned.1.call-start = ((), (), s32[]{:S(2)}) async-start(), calls=%async_computation.3 | async-start | bytes 1310720 | tf_op jit(solution)/shard_map/all_gather | solution.py:155
  8.8 8.7 %copy-start.4 = (f32[2,1024]{1,0:T(2,128)S(1)}, f32[2,1024]{1,0:T(2,128)}, u32[]{:S(2)}) copy-start(f32[2,1024]{1,0:T(2,128)} %param.19) | copy-start | bytes 24580
  17.5 25.7 %copy-start.7 = (f32[1024]{0:T(1024)S(1)}, f32[1024]{0:T(1024)}, u32[]{:S(2)}) copy-start(f32[1024]{0:T(1024)} %param.21) | copy-start | bytes 12292
  43.1 17.9 %copy-start.3 = (f32[2,3,1024]{2,0,1:T(2,128)}, f32[2,3,1024]{2,0,1:T(2,128)S(1)}, u32[]{:S(2)}) copy-start(f32[2,3,1024]{2,0,1:T(2,128)S(1)} %psum.7) | copy-start | bytes 73732
  61.0 68.0 %all-gather.10.cloned.1.call-start = ((), (), s32[]{:S(2)}) async-start(), calls=%async_computation.1 | async-start | bytes 1310720 | tf_op jit(solution)/shard_map/all_gather | solution.py:154
  66.4 2.5 copy-start.9
  66.4 2.5 copy-start.12
  68.8 106.7 %all-gather.18.cloned.1.call-start = ((), (), s32[]{:S(2)}) async-start(), calls=%async_computation.5 | async-start | bytes 2621440 | tf_op jit(solution)/shard_map/all_gather | solution.py:161
  70.7 3.4 %copy-start = (bf16[512,4096]{1,0:T(8,128)(2,1)S(1)}, bf16[512,4096]{1,0:T(8,128)(2,1)}, u32[]{:S(2)}) copy-start(bf16[512,4096]{1,0:T(8,128)(2,1)} %all-gather.12.cloned.1.call-done) | copy-start | bytes 12582916
  79.5 6.7 %copy-start.8 = (f32[64]{0:T(128)S(1)}, f32[64]{0:T(128)}, u32[]{:S(2)}) copy-start(f32[64]{0:T(128)} %param.26) | copy-start | bytes 772
  79.5 141.9 %all-gather.16.cloned.1.call-start = ((), (), s32[]{:S(2)}) async-start(), calls=%async_computation.4 | async-start | bytes 2621440 | tf_op jit(solution)/shard_map/all_gather | solution.py:160
  79.8 7.7 %copy-start.13 = (bf16[4096,512]{1,0:T(8,128)(2,1)S(1)}, bf16[4096,512]{1,0:T(8,128)(2,1)}, u32[]{:S(2)}) copy-start(bf16[4096,512]{1,0:T(8,128)(2,1)} %param.22) | copy-start | bytes 12582916
  86.2 2.4 copy-start.1
  88.6 2.8 copy-start.11
  91.9 189.7 %all-gather.20.cloned.1.call-start = ((), (), s32[]{:S(2)}) async-start(), calls=%async_computation.6 | async-start | bytes 2621440 | tf_op jit(solution)/shard_map/all_gather | solution.py:170
  257.9 0.7 copy-start.10
  258.0 1.0 copy-start.5
  258.0 1.0 copy-start.6
  258.2 23.4 %copy-start.2 = (bf16[512,1024]{1,0:T(8,128)(2,1)S(1)}, bf16[512,1024]{1,0:T(8,128)(2,1)}, u32[]{:S(2)}) copy-start(bf16[512,1024]{1,0:T(8,128)(2,1)} %param.17) | copy-start | bytes 3145732
Sparse Core Ops, SparseCore 0:
  8.9 25.2 all-gather.7
  35.8 34.8 all-gather.11
  72.3 27.8 all-gather.13
  101.6 27.3 all-gather.9
  130.4 45.0 all-gather.17
  176.9 44.4 all-gather.15
  260.2 21.3 all-gather.19
where the time goes:
time: 296 us; the launch traced here: 295 us
  waiting for transfers between devices  132 us (45%)
  matrix products  58.2 us (20%)
  local copies, waits for them, and re-layouts  38.6 us (13%)
  blocking collectives  31.4 us (11%)
  other arithmetic  19.5 us (7%)
  between operations  13.9 us (5%)
    all_gather x1, waiting for transfers between devices, local(): lax.all_gather(lat_keys, 'sp', axis=0, tiled=True)  45.9 us
    all_gather x1, waiting for transfers between devices, local(): lax.all_gather(ctx_keys, 'sp', axis=0, tiled=True)  28.8 us
    all_gather x1, waiting for transfers between devices, local(): lax.all_gather(lat_values, 'sp', axis=0, tiled=True)  25.8 us
    all_gather x1, waiting for transfers between devices, local(): lax.all_gather(head_out, 'tp', axis=1, tiled=True)  20.8 us
    psum x1, blocking collectives, local(): modulation = lax.psum(partial_mod, 'sp')  20.6 us
    dynamic_slice x12, local copies, waits for them, and re-layouts, visit_block(): lax.dynamic_slice_in_dim(value_rows, first_row, block_rows, 0)  19.1 us
    dot_general x6, matrix products, absorb(): jnp.einsum('qhmk,khv->qhmv', exponent.astype(jnp.bfloat16), value_block,...  12.7 us
    unnamed x31, local copies, waits for them, and re-layouts  10.2 us
  transfers between devices with their start and end apart: 7, of which 6 were waited for; matrix products, arithmetic and copies ran while one was open for 24% of the time, Pallas kernels for 0%

commit v1 on v0

--- a/solution.py
+++ b/solution.py
@@ -75,7 +75,7 @@
     partial_mod = jnp.dot(
         activated, mod_weight.reshape(in_rows, 3 * columns), preferred_element_type=jnp.float32
     ).reshape(2, 3, columns)
-    modulation = lax.psum(partial_mod, "sp")
+    modulation = lax.all_gather(partial_mod, "sp").sum(axis=0)
     lat_floats = latent.astype(jnp.float32)
     full_gain, full_pairs = (
         lax.all_gather(norm_gain, "tp", axis=0, tiled=True),

time: 296 us -> 296 us (level)
  waiting for transfers between devices: 132 us -> 138 us
  blocking collectives: 31.4 us -> 25.5 us
    psum x1 -> x0, blocking collectives: 20.6 us -> none  [local(): modulation = lax.psum(partial_mod, 'sp')]
    all_gather x0 -> x1, blocking collectives: none -> 14.9 us  [local(): modulation = lax.all_gather(partial_mod, 'sp').sum(axis=0)]
    all_gather x1, waiting for transfers between devices: 1.18 us -> 6.92 us  [local(): lax.all_gather(latent, 'tp', axis=1, tiled=True)]
    unnamed x31 -> x32, local copies, waits for them, and re-layouts: 10.2 us -> 10.2 us
where the time goes in v1:
time: 296 us; the launch traced here: 295 us
  waiting for transfers between devices  138 us (47%)
  matrix products  58.2 us (20%)
  local copies, waits for them, and re-layouts  38.7 us (13%)
  blocking collectives  25.5 us (9%)
  other arithmetic  19.5 us (7%)
  between operations  13.9 us (5%)
    all_gather x1, waiting for transfers between devices, local(): lax.all_gather(lat_keys, 'sp', axis=0, tiled=True)  45.9 us
    all_gather x1, waiting for transfers between devices, local(): lax.all_gather(ctx_keys, 'sp', axis=0, tiled=True)  28.8 us
    all_gather x1, waiting for transfers between devices, local(): lax.all_gather(lat_values, 'sp', axis=0, tiled=True)  25.8 us
    all_gather x1, waiting for transfers between devices, local(): lax.all_gather(head_out, 'tp', axis=1, tiled=True)  20.8 us
    dynamic_slice x12, local copies, waits for them, and re-layouts, visit_block(): lax.dynamic_slice_in_dim(value_rows, first_row, block_rows, 0)  19.1 us
    all_gather x1, blocking collectives, local(): modulation = lax.all_gather(partial_mod, 'sp').sum(axis=0)  14.9 us
    dot_general x6, matrix products, absorb(): jnp.einsum('qhmk,khv->qhmv', exponent.astype(jnp.bfloat16), value_block,...  12.7 us
    unnamed x32, local copies, waits for them, and re-layouts  10.2 us
  transfers between devices with their start and end apart: 7, of which 6 were waited for; matrix products, arithmetic and copies ran while one was open for 24% of the time, Pallas kernels for 0%

profile of v1, /device:TPU:0, one launch (start us, length us, event | category | flops | bytes accessed | tf_op | source)
XLA Modules:
  0.0 294.6 jit_solution(4935454092314804268)
XLA Ops:
  8.8 8.6 %copy.31 = bf16[1024,3,1024]{0,2,1:T(8,128)(2,1)} copy(bf16[1024,3,1024]{2,0,1:T(8,128)(2,1)} %param.20) | data formatting | bytes 12582912 | tf_op args[3]
  17.5 5.1 %fusion.27 = f32[2,3,1024]{2,0,1:T(2,128)S(1)} fusion(bf16[1024,3,1024]{0,2,1:T(8,128)(2,1)} %copy.31, f32[2,1024]{1,0:T(2,128)S(1)} %copy-done.4), kind=kOutput, calls=%fused_computation.39 | convolution fusion | flops 12593152 | bytes 6324224 | tf_op jit(solution)/shard_map/dot_general | solution.py:75
  22.6 14.9 %all-gather = f32[8,3,1024]{2,1,0:T(4,128)S(1)} all-gather(f32[2,3,1024]{2,1,0:T(4,128)S(1)} %copy.32), channel_id=2, replica_groups=mesh['grp'=2,'sp'=4,'tp'=4] {'sp'}, dimensions={0}, use_global_device_ids=true | all-gather | bytes 122880 | tf_op jit(solution)/shard_map/all_gather | solution.py:78
  37.6 5.2 %all_gather.32 = f32[4096]{0:T(1024)S(1)} all-gather(f32[1024]{0:T(1024)S(1)} %copy-done.7), channel_id=1, replica_groups=mesh['grp'=2,'sp'=4,'tp'=4] {'tp'}, dimensions={0}, use_global_device_ids=true | all-gather | bytes 20480 | tf_op jit(solution)/shard_map/all_gather | solution.py:81
  42.8 5.4 %all_gather.33 = f32[2,2,4096]{2,0,1:T(2,128)S(1)} all-gather(f32[2,2,1024]{2,0,1:T(2,128)S(1)} %copy.50), channel_id=1, replica_groups=mesh['grp'=2,'sp'=4,'tp'=4] {'tp'}, dimensions={2}, use_global_device_ids=true | all-gather | bytes 81920 | tf_op jit(solution)/shard_map/all_gather | solution.py:82
  48.2 2.1 fusion.29
  50.3 4.9 %convolution_convert_fusion.1 = bf16[256,512]{1,0:T(8,128)(2,1)} fusion(bf16[4096,512]{1,0:T(8,128)(2,1)} %param.24, bf16[256,4096]{1,0:T(8,128)(2,1)} %all-gather.9.cloned.1.call-done, f32[4096]{0:T(1024)S(1)} %bitcast.206, f32[4096]{0:T(1024)S(1)} %bitcast.208, f32[4096]{0:T(1024)S(1)} %all_gather.32, f32[256]{0:T(256)S(1)} %add_rsqrt_fusion.5), kind=kOutput, calls=%fused_computation.50 | convolution fusion | flops 1080164352 | bytes 6603776 | tf_op jit(solution)/shard_map/dot_general | solution.py:94
  55.6 4.9 %fusion.59 = (f32[256,512]{1,0:T(8,128)S(1)}, f32[256,512]{1,0:T(8,128)}) fusion(bf16[4096,512]{1,0:T(8,128)(2,1)} %param.23, bf16[256,4096]{1,0:T(8,128)(2,1)} %all-gather.9.cloned.1.call-done, f32[4096]{0:T(1024)S(1)} %bitcast.207, f32[4096]{0:T(1024)S(1)} %bitcast.209, f32[4096]{0:T(1024)S(1)} %all_gather.32, f32[256]{0:T(256)S(1)} %add_rsqrt_fusion.5), kind=kOutput, calls=%fused_computation.117 | convolution fusion | flops 1080164352 | bytes 7390208 | tf_op jit(solution)/shard_map/dot_general | solution.py:93
  61.1 1.9 multiply_convert_fusion
  63.7 6.9 %all-gather.13.cloned.1.call-done = bf16[512,4096]{1,0:T(8,128)(2,1)} async-done(((bf16[512,1024]{1,0:T(8,128)(2,1)}), bf16[512,4096]{1,0:T(8,128)(2,1)}) %all-gather.13.cloned.1.call-update) | async-done | bytes 4194320 | tf_op jit(solution)/shard_map/all_gather | solution.py:85
  70.6 3.2 %fusion.22 = f32[512]{0:T(512)S(1)} fusion(bf16[512,4096]{1,0:T(8,128)(2,1)} %all-gather.13.cloned.1.call-done), kind=kLoop, calls=%fused_computation.34 | loop fusion | flops 6290944 | bytes 4196352 | tf_op jit(solution)/shard_map/reduce_sum | solution.py:50
  74.1 5.4 %convolution_convert_fusion = bf16[512,512]{1,0:T(8,128)(2,1)} fusion(bf16[4096,512]{1,0:T(8,128)(2,1)} %param.24, bf16[512,4096]{1,0:T(8,128)(2,1)S(1)} %copy-done, f32[4096]{0:T(1024)S(1)} %bitcast.203, f32[4096]{0:T(1024)S(1)} %bitcast.200, f32[4096]{0:T(1024)S(1)} %all_gather.32, f32[512]{0:T(512)S(1)} %add_rsqrt_fusion.4), kind=kOutput, calls=%fused_computation.49 | convolution fusion | flops 2160328704 | bytes 8964096 | tf_op jit(solution)/shard_map/dot_general | solution.py:92
  79.7 6.4 %multiply_reduce_fusion = (f32[512,4,2]{0,2,1:T(2,128)S(1)}, f32[512,512]{0,1:T(8,128)S(1)}) fusion(bf16[4096,512]{1,0:T(8,128)(2,1)} %param.23, bf16[512,4096]{1,0:T(8,128)(2,1)} %all-gather.13.cloned.1.call-done, f32[4096]{0:T(1024)S(1)} %bitcast.204, f32[4096]{0:T(1024)S(1)} %bitcast.201, f32[4096]{0:T(1024)S(1)} %all_gather.32, f32[512]{0:T(512)S(1)} %add_rsqrt_fusion.4), kind=kOutput, calls=%fused_computation.64 | convolution fusion | flops 2160586752 | bytes 9504768 | tf_op jit(solution)/shard_map/dot_general | solution.py:91
  88.5 2.8 multiply_reduce_fusion.1
  92.1 8.1 %all-gather.15.cloned.1.call-done = bf16[1024,512]{1,0:T(8,128)(2,1)} async-done(((bf16[256,512]{1,0:T(8,128)(2,1)}), bf16[1024,512]{1,0:T(8,128)(2,1)}) %all-gather.15.cloned.1.call-update) | async-done | bytes 1048592 | tf_op jit(solution)/shard_map/all_gather | solution.py:155
  100.2 28.8 %all-gather.11.cloned.1.call-done = bf16[1024,512]{1,0:T(8,128)(2,1)} async-done(((bf16[256,512]{1,0:T(8,128)(2,1)}), bf16[1024,512]{1,0:T(8,128)(2,1)}) %all-gather.11.cloned.1.call-update) | async-done | bytes 1048592 | tf_op jit(solution)/shard_map/all_gather | solution.py:154
  129.0 20.6 %while.36 = (s32[]{:T(128)}, f32[512,4,2]{0,2,1:T(2,128)S(1)}, f32[512,4,2]{0,2,1:T(2,128)S(1)}, f32[512,4,2,128]{0,3,2,1:T(8,128)S(1)}, bf16[1024,512]{1,0:T(8,...) while((s32[]{:T(128)}, f32[512,4,2]{0,2,1:T(2,128)S(1)}, ...), condition=%wide.region_8.9_spmd.clone, body=%wide.region_5.8_spmd.clone.sunk | while | flops 823676928 | bytes 35389616 | solution.py:146
  129.0 2.1 constant_dynamic-slice_fusion.9
  132.1 1.3 copy.63
  133.3 2.4 bitcast_reduce_fusion.6
  135.7 1.4 fusion.96
  137.2 2.1 bitcast_add_fusion.5
  139.3 2.1 constant_dynamic-slice_fusion.9
  142.4 1.3 copy.63
  143.7 2.4 bitcast_reduce_fusion.6
  146.1 1.4 fusion.96
  147.5 2.1 bitcast_add_fusion.5
  149.7 25.8 %all-gather.19.cloned.1.call-done = bf16[2048,512]{1,0:T(8,128)(2,1)} async-done(((bf16[512,512]{1,0:T(8,128)(2,1)}), bf16[2048,512]{1,0:T(8,128)(2,1)}) %all-gather.19.cloned.1.call-update) | async-done | bytes 2097168 | tf_op jit(solution)/shard_map/all_gather | solution.py:161
  175.5 45.9 %all-gather.17.cloned.1.call-done = bf16[2048,512]{0,1:T(8,128)(2,1)} async-done(((bf16[512,512]{0,1:T(8,128)(2,1)}), bf16[2048,512]{0,1:T(8,128)(2,1)}) %all-gather.17.cloned.1.call-update) | async-done | bytes 2097168 | tf_op jit(solution)/shard_map/all_gather | solution.py:160
  221.4 36.4 %while.35 = (s32[]{:T(128)}, f32[512,4,2]{0,2,1:T(2,128)S(1)}, f32[512,4,2]{0,2,1:T(2,128)S(1)}, f32[512,4,2,128]{0,3,2,1:T(8,128)S(1)}, bf16[2048,512]{0,1:T(8,...) while((s32[]{:T(128)}, f32[512,4,2]{0,2,1:T(2,128)S(1)}, ...), condition=%wide.region_13.14_spmd, body=%wide.region_10.13_spmd.sunk | while | flops 823140352 | bytes 34341024 | solution.py:146
  221.4 1.9 constant_dynamic-slice_fusion.8
  225.6 1.3 bitcast_reduce_fusion.5
  227.0 1.4 fusion.90
  228.4 2.1 bitcast_add_fusion.4
  230.5 1.9 constant_dynamic-slice_fusion.8
  234.7 1.3 bitcast_reduce_fusion.5
  236.1 1.4 fusion.90
  237.5 2.1 bitcast_add_fusion.4
  239.6 1.9 constant_dynamic-slice_fusion.8
  243.9 1.3 bitcast_reduce_fusion.5
  245.2 1.4 fusion.90
  246.6 2.1 bitcast_add_fusion.4
  248.8 1.9 constant_dynamic-slice_fusion.8
  253.0 1.3 bitcast_reduce_fusion.5
  254.3 1.4 fusion.90
  255.7 2.1 bitcast_add_fusion.4
  260.8 20.8 %all-gather.21.cloned.1.call-done = bf16[512,2048]{0,1:T(8,128)(2,1)} async-done(((bf16[512,512]{0,1:T(8,128)(2,1)}), bf16[512,2048]{0,1:T(8,128)(2,1)}) %all-gather.21.cloned.1.call-update) | async-done | bytes 2097168 | tf_op jit(solution)/shard_map/all_gather | solution.py:170
  281.6 6.1 %add_convert_fusion = bf16[512,1024]{1,0:T(8,128)(2,1)} fusion(bf16[512,1024]{1,0:T(8,128)(2,1)S(1)} %copy-done.2, bf16[512,2048]{0,1:T(8,128)(2,1)} %all-gather.21.cloned.1.call-done, bf16[2048,1024]{1,0:T(8,128)(2,1)} %param.29, f32[1024]{0:T(1024)S(1)} %bitcast.210), kind=kOutput, calls=%fused_computation.48 | convolution fusion | flops 2149580800 | bytes 8392704 | tf_op jit(solution)/shard_map/dot_general | solution.py:169
  (110 shorter events, 22.0 us)
Async XLA Ops:
  6.5 41.7 %all-gather.9.cloned.1.call-start = ((), (), s32[]{:S(2)}) async-start(), calls=%async_computation | async-start | bytes 2621440 | tf_op jit(solution)/shard_map/all_gather | solution.py:86
  7.3 63.4 %all-gather.13.cloned.1.call-start = ((), (), s32[]{:S(2)}) async-start(), calls=%async_computation.2 | async-start | bytes 5242880 | tf_op jit(solution)/shard_map/all_gather | solution.py:85
  8.0 92.2 %all-gather.15.cloned.1.call-start = ((), (), s32[]{:S(2)}) async-start(), calls=%async_computation.3 | async-start | bytes 1310720 | tf_op jit(solution)/shard_map/all_gather | solution.py:155
  8.8 8.7 %copy-start.4 = (f32[2,1024]{1,0:T(2,128)S(1)}, f32[2,1024]{1,0:T(2,128)}, u32[]{:S(2)}) copy-start(f32[2,1024]{1,0:T(2,128)} %param.19) | copy-start | bytes 24580
  17.5 20.1 %copy-start.7 = (f32[1024]{0:T(1024)S(1)}, f32[1024]{0:T(1024)}, u32[]{:S(2)}) copy-start(f32[1024]{0:T(1024)} %param.21) | copy-start | bytes 12292
  37.5 17.7 %copy-start.3 = (f32[2,3,1024]{2,1,0:T(4,128)}, f32[2,3,1024]{2,1,0:T(4,128)S(1)}, u32[]{:S(2)}) copy-start(f32[2,3,1024]{2,1,0:T(4,128)S(1)} %reduce_sum.89) | copy-start | bytes 73732
  55.2 73.8 %all-gather.11.cloned.1.call-start = ((), (), s32[]{:S(2)}) async-start(), calls=%async_computation.1 | async-start | bytes 1310720 | tf_op jit(solution)/shard_map/all_gather | solution.py:154
  60.5 2.5 copy-start.9
  60.5 2.5 copy-start.12
  63.0 112.5 %all-gather.19.cloned.1.call-start = ((), (), s32[]{:S(2)}) async-start(), calls=%async_computation.5 | async-start | bytes 2621440 | tf_op jit(solution)/shard_map/all_gather | solution.py:161
  70.6 3.4 %copy-start = (bf16[512,4096]{1,0:T(8,128)(2,1)S(1)}, bf16[512,4096]{1,0:T(8,128)(2,1)}, u32[]{:S(2)}) copy-start(bf16[512,4096]{1,0:T(8,128)(2,1)} %all-gather.13.cloned.1.call-done) | copy-start | bytes 12582916
  79.4 6.7 %copy-start.8 = (f32[64]{0:T(128)S(1)}, f32[64]{0:T(128)}, u32[]{:S(2)}) copy-start(f32[64]{0:T(128)} %param.26) | copy-start | bytes 772
  79.5 142.0 %all-gather.17.cloned.1.call-start = ((), (), s32[]{:S(2)}) async-start(), calls=%async_computation.4 | async-start | bytes 2621440 | tf_op jit(solution)/shard_map/all_gather | solution.py:160
  79.7 7.7 %copy-start.13 = (bf16[4096,512]{1,0:T(8,128)(2,1)S(1)}, bf16[4096,512]{1,0:T(8,128)(2,1)}, u32[]{:S(2)}) copy-start(bf16[4096,512]{1,0:T(8,128)(2,1)} %param.22) | copy-start | bytes 12582916
  86.1 2.4 copy-start.1
  88.5 2.8 copy-start.11
  91.8 189.8 %all-gather.21.cloned.1.call-start = ((), (), s32[]{:S(2)}) async-start(), calls=%async_computation.6 | async-start | bytes 2621440 | tf_op jit(solution)/shard_map/all_gather | solution.py:170
  257.9 0.7 copy-start.10
  258.0 1.0 copy-start.5
  258.0 1.0 copy-start.6
  258.2 23.4 %copy-start.2 = (bf16[512,1024]{1,0:T(8,128)(2,1)S(1)}, bf16[512,1024]{1,0:T(8,128)(2,1)}, u32[]{:S(2)}) copy-start(bf16[512,1024]{1,0:T(8,128)(2,1)} %param.17) | copy-start | bytes 3145732
Sparse Core Ops, SparseCore 0:
  8.9 25.2 all-gather.8
  35.8 34.7 all-gather.12
  72.2 27.9 all-gather.14
  101.6 27.3 all-gather.10
  130.4 45.0 all-gather.18
  176.9 44.4 all-gather.16
  260.2 21.3 all-gather.20
